TPU v7x, 32 devices: a whole 2x2x4 slice. The times are simulated.
32 devices in a mesh: grp: 2 (over y), sp: 4 (over z), tp: 4 (over x, core).
Axes of the slice: x: 2, y: 2, z: 4, core: 2. Of those that a mesh axis runs over, the one named last changes fastest.
Arguments:
- stream: bfloat16 [3072, 4096], P(('grp', 'sp'), 'tp'), parts along dimension 0, may hold values from -6 to 6
- norm_gain: bfloat16 [2, 4096], replicated, may hold values from 0.099609375 to 1.8984375
- w_signal: bfloat16 [2, 4096, 1024], P(None, 'sp', 'tp'), may hold values from -0.09375 to 0.09375
- w_gate: bfloat16 [2, 4096, 1024], P(None, 'sp', 'tp'), may hold values from -0.09375 to 0.09375
- conv_taps: bfloat16 [2, 31, 1024], P(None, None, 'tp'), may hold values from -4 to 4
- conv_bias: bfloat16 [2, 1024], P(None, 'tp'), may hold values from -3 to 3
- ln_gain: bfloat16 [2, 1024], P(None, 'tp'), may hold values from 0.099609375 to 1.8984375
- ln_shift: bfloat16 [2, 1024], P(None, 'tp'), may hold values from -3 to 3
- w_out: bfloat16 [2, 1024, 4096], P(None, 'sp', 'tp'), may hold values from -0.375 to 0.375
Outputs:
- mixed_stream: bfloat16 [3072, 4096], P(('grp', 'sp'), 'tp'), parts along dimension 0
There are 2 independent parts, one for each index of `grp`. A program takes and returns all parts, laid end to end along the dimension named above; an argument that names none is the same for every part. Nothing has to cross between parts.
All inputs are finite; a program needn't handle non-finite values.
Results may differ from a plain program's by a relative error of at most 0.01.
Values may be sent and summed in bfloat16 or wider, within the bound.
A program may use at most 64 MiB of HBM per device.

v0:
```python
import jax
import jax.numpy as jnp
from jax import lax
from jax.sharding import PartitionSpec as P

C = 1024
EPS = 1e-05


def shifted(value, axis, steps):
    count = lax.axis_size(axis)
    initial, last = (max(0, -steps), min(count, count - steps))
    return lax.ppermute(value, axis, [(source, source + steps) for source in range(initial, last)])


def product(left, right):
    return jnp.dot(left, right, preferred_element_type=jnp.float32)


def shards(stream, norm_gain, w_signal, w_gate, conv_taps, conv_bias, ln_gain, ln_shift, w_out):
    fringe_rows = conv_taps.shape[1] - 1
    own_rows = stream.shape[0]
    layer_count = w_signal.shape[0]
    local_channels = w_signal.shape[2]
    whole_signal, whole_gate, whole_out = (
        lax.all_gather(w_signal, "sp", axis=1, tiled=True),
        lax.all_gather(w_gate, "sp", axis=1, tiled=True),
        lax.all_gather(w_out, "sp", axis=1, tiled=True),
    )
    current = stream
    for layer_index in range(layer_count):
        features = lax.all_gather(current, "tp", axis=1, tiled=True)
        widened = features.astype(jnp.float32)
        normed = (
            widened
            * lax.rsqrt(jnp.mean(widened * widened, axis=-1, keepdims=True) + EPS)
            * norm_gain[layer_index].astype(jnp.float32)
        ).astype(jnp.bfloat16)
        signal = product(normed, whole_signal[layer_index])
        gate_pre = product(normed, whole_gate[layer_index])
        blended = (signal * jax.nn.sigmoid(gate_pre)).astype(jnp.bfloat16)
        earlier = shifted(blended[own_rows - fringe_rows :], "sp", 1)
        padded = jnp.concatenate([earlier, blended], axis=0)
        length = padded.shape[0] - fringe_rows
        filtered = jnp.zeros((length, local_channels), jnp.float32) + conv_bias[layer_index].astype(
            jnp.float32
        )
        tap_rows = conv_taps[layer_index].astype(jnp.float32)
        for tap_index in range(fringe_rows + 1):
            filtered = filtered + tap_rows[tap_index] * padded[
                tap_index : tap_index + length
            ].astype(jnp.float32)
        totals = lax.psum((jnp.sum(filtered, axis=-1), jnp.sum(filtered * filtered, axis=-1)), "tp")
        average = totals[0][:, None] / C
        spread = totals[1][:, None] / C - average * average
        scaled = (filtered - average) * lax.rsqrt(spread + EPS) * ln_gain[layer_index].astype(
            jnp.float32
        ) + ln_shift[layer_index].astype(jnp.float32)
        activated = jax.nn.silu(scaled).astype(jnp.bfloat16)
        channels = lax.all_gather(activated, "tp", axis=1, tiled=True)
        update = product(channels, whole_out[layer_index])
        current = (current.astype(jnp.float32) + update).astype(jnp.bfloat16)
    return current


def solution(mesh):
    return jax.shard_map(
        shards,
        mesh=mesh,
        in_specs=(
            P(("grp", "sp"), "tp"),
            P(),
            P(None, "sp", "tp"),
            P(None, "sp", "tp"),
            P(None, None, "tp"),
            P(None, "tp"),
            P(None, "tp"),
            P(None, "tp"),
            P(None, "sp", "tp"),
        ),
        out_specs=P(("grp", "sp"), "tp"),
        check_vma=False,
    )
```

profile of v0, /device:TPU:0, one launch (start us, length us, event | category | flops | bytes accessed | tf_op | source)
XLA Modules:
  0.0 354.0 jit_solution(9451302702197944775)
XLA Ops:
  6.5 0.0 all-gather.6.cloned.1.call-start
  6.5 0.7 all-gather.6.cloned.1.call-update
  7.3 0.0 all-gather.10.cloned.1.call-start
  7.3 0.7 all-gather.10.cloned.1.call-update
  8.0 0.0 all-gather.8.cloned.1.call-start
  8.1 0.7 all-gather.8.cloned.1.call-update
  8.7 0.0 all-gather.12.cloned.1.call-start
  8.8 0.5 all-gather.12.cloned.1.call-update
  9.3 0.0 all-gather.14.cloned.1.call-start
  9.4 0.8 slice_convert_fusion.6
  10.1 0.8 slice_convert_fusion.5
  10.9 0.9 slice_convert_fusion
  11.8 0.8 slice_convert_fusion.2
  12.6 27.5 %all-gather.6.cloned.1.call-done = bf16[384,4096]{1,0:T(8,128)(2,1)} async-done(((bf16[384,1024]{1,0:T(8,128)(2,1)}), bf16[384,4096]{1,0:T(8,128)(2,1)}) %all-gather.6.cloned.1.call-update) | async-done | bytes 3145744 | tf_op jit(solution)/shard_map/all_gather | solution.py:32
  40.2 2.6 fusion
  42.7 79.8 %all-gather.10.cloned.1.call-done = bf16[2,4096,256]{2,1,0:T(8,128)(2,1)} async-done(((bf16[2,1024,256]{2,1,0:T(8,128)(2,1)}), bf16[2,4096,256]{2,1,0:T(8,128)(2,1)}) %all-gather.10.cloned.1.call-update) | async-done | bytes 4194320 | tf_op jit(solution)/shard_map/all_gather | solution.py:27
  122.5 0.0 copy-start
  122.5 4.5 %fusion.21 = f32[384,256]{1,0:T(8,128)} fusion(bf16[2,4096,256]{2,1,0:T(8,128)(2,1)} %all-gather.10.cloned.1.call-done, bf16[384,4096]{1,0:T(8,128)(2,1)} %all-gather.6.cloned.1.call-done, f32[4096]{0:T(1024)S(1)} %bitcast.120, f32[384]{0:T(512)S(1)} %add_rsqrt_fusion.3), kind=kOutput, calls=%fused_computation.91 | convolution fusion | flops 811892736 | bytes 5654016 | tf_op jit(solution)/shard_map/dot_general | solution.py:17
  127.0 0.0 copy-start.3
  127.0 76.4 %all-gather.8.cloned.1.call-done = bf16[2,4096,256]{2,1,0:T(8,128)(2,1)} async-done(((bf16[2,1024,256]{2,1,0:T(8,128)(2,1)}), bf16[2,4096,256]{2,1,0:T(8,128)(2,1)}) %all-gather.8.cloned.1.call-update) | async-done | bytes 4194320 | tf_op jit(solution)/shard_map/all_gather | solution.py:26
  203.3 0.0 copy-done
  203.3 2.8 fusion.23
  206.1 1.3 collective-permute-start
  207.4 0.0 copy-done.3
  207.4 1.4 collective-permute-done
  208.8 1.9 fusion.87
  210.7 5.9 %all-reduce.1 = (f32[384]{0:T(512)S(1)}, f32[384]{0:T(512)S(1)}) all-reduce(f32[384]{0:T(512)S(1)} %get-tuple-element.8, f32[384]{0:T(512)S(1)} %get-tuple-element.7), channel_id=1, replica_groups=mesh['grp'=2,'sp'=4,'tp'=4] {'tp'}, use_global_device_ids=true, to_apply=%region_4.0 | all-reduce | flops 768 | bytes 6144 | tf_op jit(solution)/shard_map/psum | solution.py:53
  216.6 0.2 multiply_convert_fusion.1
  216.8 8.8 %all_gather.24 = bf16[384,1024]{1,0:T(8,128)(2,1)S(1)} all-gather(bf16[384,256]{1,0:T(8,128)(2,1)S(1)} %multiply_convert_fusion.1), channel_id=1, replica_groups=mesh['grp'=2,'sp'=4,'tp'=4] {'tp'}, dimensions={1}, use_global_device_ids=true | all-gather | bytes 983040 | tf_op jit(solution)/shard_map/all_gather | solution.py:60
  225.6 58.4 %all-gather.12.cloned.1.call-done = bf16[2,1024,1024]{2,1,0:T(8,128)(2,1)} async-done(((bf16[2,256,1024]{2,1,0:T(8,128)(2,1)}), bf16[2,1024,1024]{2,1,0:T(8,128)(2,1)}) %all-gather.12.cloned.1.call-update) | async-done | bytes 4194320 | tf_op jit(solution)/shard_map/all_gather | solution.py:28
  284.0 3.6 %add_convert_fusion.1 = bf16[384,1024]{1,0:T(8,128)(2,1)} fusion(bf16[384,1024]{1,0:T(8,128)(2,1)} %param.9, bf16[384,1024]{1,0:T(8,128)(2,1)S(1)} %all_gather.24, bf16[2,1024,1024]{2,1,0:T(8,128)(2,1)} %all-gather.12.cloned.1.call-done), kind=kOutput, calls=%fused_computation.81 | convolution fusion | flops 806486016 | bytes 4456448 | tf_op jit(solution)/shard_map/dot_general | solution.py:17
  287.6 0.0 all-gather.14.cloned.1.call-update
  287.7 27.1 %all-gather.14.cloned.1.call-done = bf16[384,4096]{1,0:T(8,128)(2,1)} async-done(((bf16[384,1024]{1,0:T(8,128)(2,1)}), bf16[384,4096]{1,0:T(8,128)(2,1)}) %all-gather.14.cloned.1.call-update) | async-done | bytes 3145744 | tf_op jit(solution)/shard_map/all_gather | solution.py:32
  314.8 2.6 fusion.3
  317.4 0.0 copy-start.1
  317.4 0.0 copy-start.4
  317.4 3.7 %fusion.19 = f32[384,256]{1,0:T(8,128)S(1)} fusion(bf16[2,4096,256]{2,1,0:T(8,128)(2,1)} %all-gather.10.cloned.1.call-done, bf16[384,4096]{1,0:T(8,128)(2,1)} %all-gather.14.cloned.1.call-done, f32[4096]{0:T(1024)S(1)} %bitcast.118, f32[384]{0:T(512)S(1)} %add_rsqrt_fusion.1), kind=kOutput, calls=%fused_computation.89 | convolution fusion | flops 811892736 | bytes 5654016 | tf_op jit(solution)/shard_map/dot_general | solution.py:17
  321.2 0.0 copy-done.1
  321.2 1.0 copy-done.4
  322.1 0.0 copy-start.2
  322.1 1.0 fusion.22
  323.2 3.4 collective-permute-start.1
  326.6 1.4 collective-permute-done.1
  328.0 1.9 fusion.86
  329.9 5.9 %all-reduce = (f32[384]{0:T(512)S(1)}, f32[384]{0:T(512)S(1)}) all-reduce(f32[384]{0:T(512)S(1)} %get-tuple-element.6, f32[384]{0:T(512)S(1)} %get-tuple-element.5), channel_id=1, replica_groups=mesh['grp'=2,'sp'=4,'tp'=4] {'tp'}, use_global_device_ids=true, to_apply=%region_9.10 | all-reduce | flops 768 | bytes 6144 | tf_op jit(solution)/shard_map/psum | solution.py:53
  335.9 0.2 multiply_convert_fusion
  336.1 7.9 %all_gather.27 = bf16[384,1024]{1,0:T(8,128)(2,1)S(1)} all-gather(bf16[384,256]{1,0:T(8,128)(2,1)S(1)} %multiply_convert_fusion), channel_id=1, replica_groups=mesh['grp'=2,'sp'=4,'tp'=4] {'tp'}, dimensions={1}, use_global_device_ids=true | all-gather | bytes 983040 | tf_op jit(solution)/shard_map/all_gather | solution.py:60
  344.0 0.0 copy-done.2
  344.1 3.5 add_convert_fusion
  (11 shorter events, 0.1 us)
Async XLA Ops:
  6.5 33.6 %all-gather.6.cloned.1.call-start = ((), (), s32[]{:S(2)}) async-start(), calls=%async_computation | async-start | bytes 3932160 | tf_op jit(solution)/shard_map/all_gather | solution.py:32
  7.3 115.2 %all-gather.10.cloned.1.call-start = ((), (), s32[]{:S(2)}) async-start(), calls=%async_computation.2 | async-start | bytes 5242880 | tf_op jit(solution)/shard_map/all_gather | solution.py:27
  8.0 195.3 %all-gather.8.cloned.1.call-start = ((), (), s32[]{:S(2)}) async-start(), calls=%async_computation.1 | async-start | bytes 5242880 | tf_op jit(solution)/shard_map/all_gather | solution.py:26
  8.7 275.3 %all-gather.12.cloned.1.call-start = ((), (), s32[]{:S(2)}) async-start(), calls=%async_computation.3 | async-start | bytes 5242880 | tf_op jit(solution)/shard_map/all_gather | solution.py:28
  9.3 305.5 %all-gather.14.cloned.1.call-start = ((), (), s32[]{:S(2)}) async-start(), calls=%async_computation.4 | async-start | bytes 3932160 | tf_op jit(solution)/shard_map/all_gather | solution.py:32
  122.5 80.8 %copy-start = (bf16[384,4096]{1,0:T(8,128)(2,1)S(1)}, bf16[384,4096]{1,0:T(8,128)(2,1)}, u32[]{:S(2)}) copy-start(bf16[384,4096]{1,0:T(8,128)(2,1)} %all-gather.6.cloned.1.call-done) | copy-start | bytes 9437188
  127.0 80.4 %copy-start.3 = (bf16[2,256]{1,0:T(2,128)(2,1)S(1)}, bf16[2,256]{1,0:T(2,128)(2,1)}, u32[]{:S(2)}) copy-start(bf16[2,256]{1,0:T(2,128)(2,1)} %param.16) | copy-start | bytes 3076
  206.1 2.7 collective-permute-start
  317.4 3.8 %copy-start.1 = (bf16[384,4096]{1,0:T(8,128)(2,1)S(1)}, bf16[384,4096]{1,0:T(8,128)(2,1)}, u32[]{:S(2)}) copy-start(bf16[384,4096]{1,0:T(8,128)(2,1)} %all-gather.14.cloned.1.call-done) | copy-start | bytes 9437188
  317.4 4.7 %copy-start.4 = (bf16[2,4096,256]{2,1,0:T(8,128)(2,1)S(1)}, bf16[2,4096,256]{2,1,0:T(8,128)(2,1)}, u32[]{:S(2)}) copy-start(bf16[2,4096,256]{2,1,0:T(8,128)(2,1)} %all-gather.8.cloned.1.call-done) | copy-start | bytes 12582916
  322.1 21.9 %copy-start.2 = (bf16[384,1024]{1,0:T(8,128)(2,1)S(1)}, bf16[384,1024]{1,0:T(8,128)(2,1)}, u32[]{:S(2)}) copy-start(bf16[384,1024]{1,0:T(8,128)(2,1)} %add_convert_fusion.1) | copy-start | bytes 2359300
  323.2 4.8 %collective-permute-start.1 = (bf16[30,256]{1,0:T(8,128)(2,1)S(1)}, bf16[30,256]{1,0:T(8,128)(2,1)S(1)}, u32[]{:S(2)}, u32[]{:S(2)}) collective-permute-start(bf16[30,256]{1,0:T(8,128)(2,1)S(1)} %slice.718), channel_id=1, source_target_pairs={{0,4},{4,8},{8,12},{1,5},{5,9},{9,13},{2,6},{6,10},{10,14},{3,7},{... | collective-permute-start | bytes 46088 | tf_op jit(solution)/shard_map/ppermute | solution.py:13
Sparse Core Ops, SparseCore 0:
  8.9 31.2 all-gather.5
  41.7 80.7 all-gather.9
  124.1 79.2 all-gather.7
  204.8 79.2 all-gather.11
  287.8 26.9 all-gather.13
where the time goes:
time: 355 us; the launch traced here: 354 us
  waiting for transfers between devices  275 us (77%)
  blocking collectives  28.5 us (8%)
  matrix products  19.1 us (5%)
  between operations  13.3 us (4%)
  other arithmetic  12.7 us (4%)
  starting transfers between devices  4.83 us (1%)
    all_gather x1, waiting for transfers between devices, shards(): lax.all_gather(w_gate, 'sp', axis=1, tiled=True)  79.8 us
    all_gather x1, waiting for transfers between devices, shards(): lax.all_gather(w_signal, 'sp', axis=1, tiled=True)  76.4 us
    all_gather x1, waiting for transfers between devices, shards(): lax.all_gather(w_out, 'sp', axis=1, tiled=True)  58.4 us
    all_gather x2, waiting for transfers between devices, shards(): features = lax.all_gather(current, 'tp', axis=1, tiled=True)  54.7 us
    dot_general x6, matrix products, product(): return jnp.dot(left, right, preferred_element_type=jnp.float32)  19.1 us
    all_gather x2, blocking collectives, shards(): channels = lax.all_gather(activated, 'tp', axis=1, tiled=True)  16.7 us
    psum x2, blocking collectives, shards(): lax.psum((jnp.sum(filtered, axis=-1), jnp.sum(filtered * filtered, axis=-...  11.8 us
  transfers between devices with their start and end apart: 7, of which 7 were waited for; matrix products, arithmetic and copies ran while one was open for 4% of the time, Pallas kernels for 0%

commit v1 on v0

--- a/solution.py
+++ b/solution.py
@@ -2,6 +2,7 @@
 import jax.numpy as jnp
 from jax import lax
 from jax.sharding import PartitionSpec as P
+from jax.lax import axis_index, ppermute, psum
 
 C = 1024
 EPS = 1e-05
@@ -29,7 +30,21 @@
     )
     current = stream
     for layer_index in range(layer_count):
-        features = lax.all_gather(current, "tp", axis=1, tiled=True)
+
+        def press_slots(point):
+            ax_name = "tp"
+            num = psum(1, ax_name)
+            passed = [(h - 1, h) for h in range(1, num)] + [(num - 1, 0)]
+            part_now = point
+            kept_rows = [part_now]
+            for _ in range(num - 1):
+                part_now = ppermute(part_now, ax_name, passed)
+                kept_rows += [part_now]
+            new = jnp.concatenate([*reversed(kept_rows)], axis=1)
+            tile_out = jnp.roll(new, shift=(axis_index(ax_name) + 1) * part_now.shape[1], axis=1)
+            return tile_out
+
+        features = press_slots(current)
         widened = features.astype(jnp.float32)
         normed = (
             widened

time: 355 us -> 330 us (0.930)
  waiting for transfers between devices: 275 us -> 249 us
  other arithmetic: 12.7 us -> 19.1 us
  matrix products: 19.1 us -> 14.3 us
    ppermute x0 -> x6, waiting for transfers between devices: none -> 65.2 us  [press_slots(): part_now = ppermute(part_now, ax_name, passed)]
    all_gather x2 -> x0, waiting for transfers between devices: 54.7 us -> none  [shards(): features = lax.all_gather(current, 'tp', axis=1, tiled=True)]
    all_gather x1, waiting for transfers between devices: 79.8 us -> 43.2 us  [shards(): lax.all_gather(w_gate, 'sp', axis=1, tiled=True)]
    reduce_sum x2, other arithmetic: 5.16 us -> 11.5 us  [shards(): jnp.mean(widened * widened, axis=-1, keepdims=True) + EPS]
    dot_general x6, matrix products: 19.1 us -> 14.3 us  [product(): return jnp.dot(left, right, preferred_element_type=jnp.float32)]
  transfers between devices with their start and end apart: 7 -> 11, of which waited for: 7 -> 11; matrix products, arithmetic and copies ran while one was open for 4% -> 5% of each run, Pallas kernels for 0% -> 0%
where the time goes in v1:
time: 330 us; the launch traced here: 329 us
  waiting for transfers between devices  249 us (75%)
  blocking collectives  29.2 us (9%)
  other arithmetic  19.1 us (6%)
  matrix products  14.3 us (4%)
  between operations  13.3 us (4%)
  starting transfers between devices  3.49 us (1%)
    all_gather x1, waiting for transfers between devices, shards(): lax.all_gather(w_signal, 'sp', axis=1, tiled=True)  77.4 us
    ppermute x6, waiting for transfers between devices, press_slots(): part_now = ppermute(part_now, ax_name, passed)  65.2 us
    all_gather x1, waiting for transfers between devices, shards(): lax.all_gather(w_out, 'sp', axis=1, tiled=True)  58.6 us
    all_gather x1, waiting for transfers between devices, shards(): lax.all_gather(w_gate, 'sp', axis=1, tiled=True)  43.2 us
    all_gather x2, blocking collectives, shards(): channels = lax.all_gather(activated, 'tp', axis=1, tiled=True)  17.6 us
    dot_general x6, matrix products, product(): return jnp.dot(left, right, preferred_element_type=jnp.float32)  14.3 us
    reduce_sum x2, other arithmetic, shards(): jnp.mean(widened * widened, axis=-1, keepdims=True) + EPS  11.5 us
    psum x2, blocking collectives, shards(): lax.psum((jnp.sum(filtered, axis=-1), jnp.sum(filtered * filtered, axis=-...  11.5 us
  transfers between devices with their start and end apart: 11, of which 11 were waited for; matrix products, arithmetic and copies ran while one was open for 5% of the time, Pallas kernels for 0%

profile of v1, /device:TPU:0, one launch (start us, length us, event | category | flops | bytes accessed | tf_op | source)
XLA Modules:
  0.0 329.3 jit_solution(5296614960775955543)
XLA Ops:
  6.5 0.0 all-gather.6.cloned.1.call-start
  6.5 0.7 all-gather.6.cloned.1.call-update
  7.3 0.0 all-gather.4.cloned.1.call-start
  7.3 0.7 all-gather.4.cloned.1.call-update
  8.0 0.0 all-gather.8.cloned.1.call-start
  8.1 0.5 collective-permute-start
  8.6 0.1 all-gather.8.cloned.1.call-update
  8.7 0.8 slice_convert_fusion.6
  9.5 10.9 %collective-permute-done = bf16[384,1024]{1,0:T(8,128)(2,1)S(1)} collective-permute-done((bf16[384,1024]{1,0:T(8,128)(2,1)}, bf16[384,1024]{1,0:T(8,128)(2,1)S(1)}, u32[]{:S(2)}, u32[]{:S(2)}) %collective-permute-start) | collective-permute-done | bytes 786464 | tf_op jit(solution)/shard_map/ppermute | solution.py:41
  20.4 0.0 copy-start
  20.4 0.0 collective-permute-start.1
  20.4 0.8 slice_convert_fusion.5
  21.2 0.9 slice_convert_fusion
  22.1 9.7 %collective-permute-done.1 = bf16[384,1024]{1,0:T(8,128)(2,1)S(1)} collective-permute-done((bf16[384,1024]{1,0:T(8,128)(2,1)S(1)}, bf16[384,1024]{1,0:T(8,128)(2,1)S(1)}, u32[]{:S(2)}, u32[]{:S(2)}) %collective-permute-start.1) | collective-permute-done | bytes 786464 | tf_op jit(solution)/shard_map/ppermute | solution.py:41
  31.8 0.0 copy-start.1
  31.8 0.0 collective-permute-start.2
  31.8 0.8 slice_convert_fusion.2
  32.6 0.0 copy-done
  32.7 0.1 copy-done.1
  32.8 10.5 %collective-permute-done.2 = bf16[384,1024]{1,0:T(8,128)(2,1)S(1)} collective-permute-done((bf16[384,1024]{1,0:T(8,128)(2,1)S(1)}, bf16[384,1024]{1,0:T(8,128)(2,1)S(1)}, u32[]{:S(2)}, u32[]{:S(2)}) %collective-permute-start.2) | collective-permute-done | bytes 786464 | tf_op jit(solution)/shard_map/ppermute | solution.py:41
  43.2 6.0 %fusion = (f32[384]{0:T(512)S(1)}, bf16[384,4096]{1,0:T(8,128)(2,1)S(1)}) fusion(s32[]{:T(128)S(6)} %select_n.13, bf16[384,1024]{1,0:T(8,128)(2,1)} %param.11, bf16[384,1024]{1,0:T(8,128)(2,1)} %copy-done, bf16[384,1024]{1,0:T(8,128)(2,1)} %copy-done.1, bf16[384,1024]{1,0:T(8,128)(2,1)S(1)} %collective-permute-done.2), kind=kLoop, calls=%fused_computation.4 | loop fusion | flops 29884032 | bytes 6292996 | tf_op jit(solution)/shard_map/reduce_sum | solution.py:51
  49.2 43.2 %all-gather.6.cloned.1.call-done = bf16[2,4096,256]{2,1,0:T(8,128)(2,1)} async-done(((bf16[2,1024,256]{2,1,0:T(8,128)(2,1)}), bf16[2,4096,256]{2,1,0:T(8,128)(2,1)}) %all-gather.6.cloned.1.call-update) | async-done | bytes 4194320 | tf_op jit(solution)/shard_map/all_gather | solution.py:28
  92.4 3.4 %fusion.35 = f32[384,256]{1,0:T(8,128)} fusion(bf16[2,4096,256]{2,1,0:T(8,128)(2,1)} %all-gather.6.cloned.1.call-done, bf16[384,4096]{1,0:T(8,128)(2,1)S(1)} %get-tuple-element.19, f32[4096]{0:T(1024)S(1)} %bitcast.120, f32[384]{0:T(512)S(1)} %add_rsqrt_fusion.3), kind=kOutput, calls=%fused_computation.121 | convolution fusion | flops 811892736 | bytes 5654016 | tf_op jit(solution)/shard_map/dot_general | solution.py:18
  95.8 0.0 copy-start.2
  95.8 77.4 %all-gather.4.cloned.1.call-done = bf16[2,4096,256]{2,1,0:T(8,128)(2,1)} async-done(((bf16[2,1024,256]{2,1,0:T(8,128)(2,1)}), bf16[2,4096,256]{2,1,0:T(8,128)(2,1)}) %all-gather.4.cloned.1.call-update) | async-done | bytes 4194320 | tf_op jit(solution)/shard_map/all_gather | solution.py:27
  173.2 2.7 fusion.37
  175.9 1.3 collective-permute-start.3
  177.2 0.0 copy-done.2
  177.2 1.4 collective-permute-done.3
  178.6 1.9 fusion.101
  180.5 5.9 %all-reduce.1 = (f32[384]{0:T(512)S(1)}, f32[384]{0:T(512)S(1)}) all-reduce(f32[384]{0:T(512)S(1)} %get-tuple-element.9, f32[384]{0:T(512)S(1)} %get-tuple-element.8), channel_id=1, replica_groups=mesh['grp'=2,'sp'=4,'tp'=4] {'tp'}, use_global_device_ids=true, to_apply=%region_4.6 | all-reduce | flops 768 | bytes 6144 | tf_op jit(solution)/shard_map/psum | solution.py:68
  186.4 0.2 multiply_convert_fusion.1
  186.6 8.8 %all_gather.17 = bf16[384,1024]{1,0:T(8,128)(2,1)S(1)} all-gather(bf16[384,256]{1,0:T(8,128)(2,1)S(1)} %multiply_convert_fusion.1), channel_id=1, replica_groups=mesh['grp'=2,'sp'=4,'tp'=4] {'tp'}, dimensions={1}, use_global_device_ids=true | all-gather | bytes 983040 | tf_op jit(solution)/shard_map/all_gather | solution.py:75
  195.4 58.6 %all-gather.8.cloned.1.call-done = bf16[2,1024,1024]{2,1,0:T(8,128)(2,1)} async-done(((bf16[2,256,1024]{2,1,0:T(8,128)(2,1)}), bf16[2,1024,1024]{2,1,0:T(8,128)(2,1)}) %all-gather.8.cloned.1.call-update) | async-done | bytes 4194320 | tf_op jit(solution)/shard_map/all_gather | solution.py:29
  254.1 2.7 add_convert_fusion.1
  256.8 0.0 copy-start.3
  256.8 0.1 collective-permute-start.4
  256.9 11.4 %collective-permute-done.4 = bf16[384,1024]{1,0:T(8,128)(2,1)S(1)} collective-permute-done((bf16[384,1024]{1,0:T(8,128)(2,1)S(1)}, bf16[384,1024]{1,0:T(8,128)(2,1)S(1)}, u32[]{:S(2)}, u32[]{:S(2)}) %collective-permute-start.4) | collective-permute-done | bytes 786464 | tf_op jit(solution)/shard_map/ppermute | solution.py:41
  268.3 0.0 collective-permute-start.5
  268.3 11.4 %collective-permute-done.5 = bf16[384,1024]{1,0:T(8,128)(2,1)S(1)} collective-permute-done((bf16[384,1024]{1,0:T(8,128)(2,1)S(1)}, bf16[384,1024]{1,0:T(8,128)(2,1)S(1)}, u32[]{:S(2)}, u32[]{:S(2)}) %collective-permute-start.5) | collective-permute-done | bytes 786464 | tf_op jit(solution)/shard_map/ppermute | solution.py:41
  279.7 0.0 collective-permute-start.6
  279.7 11.4 %collective-permute-done.6 = bf16[384,1024]{1,0:T(8,128)(2,1)S(1)} collective-permute-done((bf16[384,1024]{1,0:T(8,128)(2,1)S(1)}, bf16[384,1024]{1,0:T(8,128)(2,1)S(1)}, u32[]{:S(2)}, u32[]{:S(2)}) %collective-permute-start.6) | collective-permute-done | bytes 786464 | tf_op jit(solution)/shard_map/ppermute | solution.py:41
  291.1 5.6 %fusion.3 = (f32[384]{0:T(512)S(1)}, bf16[384,4096]{1,0:T(8,128)(2,1)S(1)}) fusion(s32[]{:T(128)S(6)} %select_n.13, bf16[384,1024]{1,0:T(8,128)(2,1)S(1)} %add_convert_fusion.1, bf16[384,1024]{1,0:T(8,128)(2,1)S(1)} %collective-permute-done.4, bf16[384,1024]{1,0:T(8,128)(2,1)S(1)} %collective-permute-done.5, bf16[384,1024]{1,0:T(8,128)(2,1)S(1)} %collective-permute-done.6), kind=kLoop, calls=%fused_computation.7 | loop fusion | flops 29884032 | bytes 6292996 | tf_op jit(solution)/shard_map/reduce_sum | solution.py:51
  296.7 0.0 copy-done.3
  296.7 0.0 copy-start.4
  296.7 1.1 fusion.33
  297.8 1.1 copy-done.4
  298.9 1.0 fusion.36
  300.0 1.5 collective-permute-start.7
  301.5 1.2 collective-permute-done.7
  302.7 1.9 fusion.100
  304.6 5.7 %all-reduce = (f32[384]{0:T(512)S(1)}, f32[384]{0:T(512)S(1)}) all-reduce(f32[384]{0:T(512)S(1)} %get-tuple-element.7, f32[384]{0:T(512)S(1)} %get-tuple-element.6), channel_id=1, replica_groups=mesh['grp'=2,'sp'=4,'tp'=4] {'tp'}, use_global_device_ids=true, to_apply=%region_9.11 | all-reduce | flops 768 | bytes 6144 | tf_op jit(solution)/shard_map/psum | solution.py:68
  310.3 0.2 multiply_convert_fusion
  310.5 8.8 %all_gather.19 = bf16[384,1024]{1,0:T(8,128)(2,1)S(1)} all-gather(bf16[384,256]{1,0:T(8,128)(2,1)S(1)} %multiply_convert_fusion), channel_id=1, replica_groups=mesh['grp'=2,'sp'=4,'tp'=4] {'tp'}, dimensions={1}, use_global_device_ids=true | all-gather | bytes 983040 | tf_op jit(solution)/shard_map/all_gather | solution.py:75
  319.3 3.5 %add_convert_fusion = bf16[384,1024]{1,0:T(8,128)(2,1)} fusion(bf16[384,1024]{1,0:T(8,128)(2,1)S(1)} %add_convert_fusion.1, bf16[384,1024]{1,0:T(8,128)(2,1)S(1)} %all_gather.19, bf16[2,1024,1024]{2,1,0:T(8,128)(2,1)} %all-gather.8.cloned.1.call-done), kind=kOutput, calls=%fused_computation.110 | convolution fusion | flops 806486016 | bytes 4456448 | tf_op jit(solution)/shard_map/dot_general | solution.py:18
  (11 shorter events, 0.1 us)
Async XLA Ops:
  6.5 85.9 %all-gather.6.cloned.1.call-start = ((), (), s32[]{:S(2)}) async-start(), calls=%async_computation.1 | async-start | bytes 5242880 | tf_op jit(solution)/shard_map/all_gather | solution.py:28
  7.3 166.0 %all-gather.4.cloned.1.call-start = ((), (), s32[]{:S(2)}) async-start(), calls=%async_computation | async-start | bytes 5242880 | tf_op jit(solution)/shard_map/all_gather | solution.py:27
  8.0 246.1 %all-gather.8.cloned.1.call-start = ((), (), s32[]{:S(2)}) async-start(), calls=%async_computation.2 | async-start | bytes 5242880 | tf_op jit(solution)/shard_map/all_gather | solution.py:29
  8.1 12.3 %collective-permute-start = (bf16[384,1024]{1,0:T(8,128)(2,1)}, bf16[384,1024]{1,0:T(8,128)(2,1)S(1)}, u32[]{:S(2)}, u32[]{:S(2)}) collective-permute-start(bf16[384,1024]{1,0:T(8,128)(2,1)} %param.11), channel_id=1, source_target_pairs={{0,1},{1,2},{2,3},{3,0},{4,5},{5,6},{6,7},{7,4},{8,9},{9,10},{10,1... | collective-permute-start | bytes 2359304 | tf_op jit(solution)/shard_map/ppermute | solution.py:41
  20.4 12.3 %copy-start = (bf16[384,1024]{1,0:T(8,128)(2,1)}, bf16[384,1024]{1,0:T(8,128)(2,1)S(1)}, u32[]{:S(2)}) copy-start(bf16[384,1024]{1,0:T(8,128)(2,1)S(1)} %collective-permute-done) | copy-start | bytes 2359300
  20.4 11.4 %collective-permute-start.1 = (bf16[384,1024]{1,0:T(8,128)(2,1)S(1)}, bf16[384,1024]{1,0:T(8,128)(2,1)S(1)}, u32[]{:S(2)}, u32[]{:S(2)}) collective-permute-start(bf16[384,1024]{1,0:T(8,128)(2,1)S(1)} %collective-permute-done), channel_id=1, source_target_pairs={{0,1},{1,2},{2,3},{3,0},{4,5},{5,6},{6,7},{7,4},{8,9},{9,10},{10,1... | collective-permute-start | bytes 2359304 | tf_op jit(solution)/shard_map/ppermute | solution.py:41
  31.8 1.0 copy-start.1
  31.8 11.4 %collective-permute-start.2 = (bf16[384,1024]{1,0:T(8,128)(2,1)S(1)}, bf16[384,1024]{1,0:T(8,128)(2,1)S(1)}, u32[]{:S(2)}, u32[]{:S(2)}) collective-permute-start(bf16[384,1024]{1,0:T(8,128)(2,1)S(1)} %collective-permute-done.1), channel_id=1, source_target_pairs={{0,1},{1,2},{2,3},{3,0},{4,5},{5,6},{6,7},{7,4},{8,9},{9,10},{10,1... | collective-permute-start | bytes 2359304 | tf_op jit(solution)/shard_map/ppermute | solution.py:41
  95.8 81.4 %copy-start.2 = (bf16[2,256]{1,0:T(2,128)(2,1)S(1)}, bf16[2,256]{1,0:T(2,128)(2,1)}, u32[]{:S(2)}) copy-start(bf16[2,256]{1,0:T(2,128)(2,1)} %param.18) | copy-start | bytes 3076
  175.9 2.7 collective-permute-start.3
  256.8 39.9 %copy-start.3 = (bf16[2,4096,256]{2,1,0:T(8,128)(2,1)S(1)}, bf16[2,4096,256]{2,1,0:T(8,128)(2,1)}, u32[]{:S(2)}) copy-start(bf16[2,4096,256]{2,1,0:T(8,128)(2,1)} %all-gather.6.cloned.1.call-done) | copy-start | bytes 12582916
  256.8 11.5 %collective-permute-start.4 = (bf16[384,1024]{1,0:T(8,128)(2,1)S(1)}, bf16[384,1024]{1,0:T(8,128)(2,1)S(1)}, u32[]{:S(2)}, u32[]{:S(2)}) collective-permute-start(bf16[384,1024]{1,0:T(8,128)(2,1)S(1)} %add_convert_fusion.1), channel_id=1, source_target_pairs={{0,1},{1,2},{2,3},{3,0},{4,5},{5,6},{6,7},{7,4},{8,9},{9,10},{10,1... | collective-permute-start | bytes 2359304 | tf_op jit(solution)/shard_map/ppermute | solution.py:41
  268.3 11.4 %collective-permute-start.5 = (bf16[384,1024]{1,0:T(8,128)(2,1)S(1)}, bf16[384,1024]{1,0:T(8,128)(2,1)S(1)}, u32[]{:S(2)}, u32[]{:S(2)}) collective-permute-start(bf16[384,1024]{1,0:T(8,128)(2,1)S(1)} %collective-permute-done.4), channel_id=1, source_target_pairs={{0,1},{1,2},{2,3},{3,0},{4,5},{5,6},{6,7},{7,4},{8,9},{9,10},{10,1... | collective-permute-start | bytes 2359304 | tf_op jit(solution)/shard_map/ppermute | solution.py:41
  279.7 11.4 %collective-permute-start.6 = (bf16[384,1024]{1,0:T(8,128)(2,1)S(1)}, bf16[384,1024]{1,0:T(8,128)(2,1)S(1)}, u32[]{:S(2)}, u32[]{:S(2)}) collective-permute-start(bf16[384,1024]{1,0:T(8,128)(2,1)S(1)} %collective-permute-done.5), channel_id=1, source_target_pairs={{0,1},{1,2},{2,3},{3,0},{4,5},{5,6},{6,7},{7,4},{8,9},{9,10},{10,1... | collective-permute-start | bytes 2359304 | tf_op jit(solution)/shard_map/ppermute | solution.py:41
  296.7 2.2 copy-start.4
  300.0 2.7 collective-permute-start.7
Sparse Core Ops, SparseCore 0:
  8.9 83.4 all-gather.5
  94.0 79.2 all-gather.3
  174.8 79.2 all-gather.7
